TPU v7x, 32 devices: a whole 2x2x4 slice. The times are simulated.
32 devices in a mesh: sp: 8 (over z, y), dp: 4 (over x, core).
Axes of the slice: x: 2, y: 2, z: 4, core: 2. Of those that a mesh axis runs over, the one named last changes fastest.
Arguments:
- query: bfloat16 [4, 1536, 3072], P('dp', 'sp'), may hold values from -18 to 18
- latent: bfloat16 [4, 1536, 1024], P('dp', 'sp'), may hold values from -6 to 6
- rope_key: bfloat16 [4, 1536, 32], P('dp', 'sp'), may hold values from -5 to 5
- latent_norm_gain: float32 [1024], replicated, may hold values from 0.1 to 1.9
- key_up_matrix: bfloat16 [2048, 1024], P('dp'), may hold values from -0.1875 to 0.1875
- value_up_matrix: bfloat16 [2048, 1024], P('dp'), may hold values from -0.1875 to 0.1875
- out_grad: bfloat16 [4, 1536, 2048], P('dp', 'sp'), may hold values from -6 to 6
Outputs:
- query_grad: bfloat16 [4, 1536, 3072], P('dp', 'sp')
- latent_grad: float32 [4, 1536, 1024], P('dp', 'sp')
- rope_key_grad: float32 [4, 1536, 32], P('dp', 'sp')
- key_weight_grad: float32 [2048, 1024], P('dp')
- value_weight_grad: float32 [2048, 1024], P('dp')
- gain_grad: float32 [1024], replicated
All inputs are finite; a program needn't handle non-finite values.
Results may differ from a plain program's by a relative error of at most 0.011.
Values may be sent and summed in bfloat16 or wider, within the bound.
A program may use at most 256 MiB of HBM per device.

v0:
```python
import jax
import jax.numpy as jnp
from jax import lax
from jax.sharding import PartitionSpec as P

ATTENTION_HEADS = 32
PLAIN_HEAD_WIDTH = 64
ROPE = 32
VALUE_HEAD_WIDTH = 64
SPAN = 64
eps = 1e-06
rope_base = 10000.0


def rotate(values, cosine, sine):
    half = values.shape[-1] // 2
    first = values[..., :half]
    second = values[..., half:]
    return jnp.concatenate(
        [first * cosine - second * sine, second * cosine + first * sine], axis=-1
    )


def angles(length, width):
    inverse = 1.0 / rope_base ** (jnp.arange(0, width, 2, dtype=jnp.float32) / width)
    turned = jnp.arange(length, dtype=jnp.float32)[:, None] * inverse[None, :]
    return (jnp.cos(turned), jnp.sin(turned))


def attend_backward(arrived, rope_full):
    f32 = jnp.float32
    bf16 = jnp.bfloat16
    length = arrived.shape[0]
    local_heads = arrived.shape[1]
    width = PLAIN_HEAD_WIDTH + ROPE
    scale = width ** (-0.5)
    block = 512
    cosine, sine = angles(length, ROPE)
    neg = jnp.finfo(f32).min
    q_nope = arrived[:, :, :PLAIN_HEAD_WIDTH]
    q_rope = rotate(
        arrived[:, :, PLAIN_HEAD_WIDTH:width].astype(f32), cosine[:, None, :], sine[:, None, :]
    ).astype(bf16)
    key_nope = arrived[:, :, width : width + PLAIN_HEAD_WIDTH]
    values = arrived[:, :, width + PLAIN_HEAD_WIDTH : width + PLAIN_HEAD_WIDTH + VALUE_HEAD_WIDTH]
    d_out = arrived[:, :, width + PLAIN_HEAD_WIDTH + VALUE_HEAD_WIDTH :]
    k_rope = rotate(rope_full.astype(f32), cosine, sine).astype(bf16)
    dk_nope = jnp.zeros((length, local_heads, PLAIN_HEAD_WIDTH), f32)
    dk_rope = jnp.zeros((length, ROPE), f32)
    d_vals = jnp.zeros((length, local_heads, VALUE_HEAD_WIDTH), f32)
    dq_parts = []
    for begin in range(0, length, block):
        end = begin + block
        qn = q_nope[begin:end]
        qr = q_rope[begin:end]
        go = d_out[begin:end]
        scores = jnp.einsum("qhd,khd->hqk", qn, key_nope[:end], preferred_element_type=f32)
        scores = (
            scores + jnp.einsum("qhd,kd->hqk", qr, k_rope[:end], preferred_element_type=f32)
        ) * scale
        q_seg = jnp.arange(begin, end) // SPAN
        k_seg = jnp.arange(end) // SPAN
        allowed = k_seg[None, :] <= q_seg[:, None]
        scores = jnp.where(allowed[None], scores, neg)
        probs = jax.nn.softmax(scores, axis=-1)
        d_probs = jnp.einsum("qhd,khd->hqk", go, values[:end], preferred_element_type=f32)
        d_scores = probs * (d_probs - jnp.sum(probs * d_probs, axis=-1, keepdims=True))
        ds_b = d_scores.astype(bf16)
        p_b = probs.astype(bf16)
        dq_n = jnp.einsum("hqk,khd->qhd", ds_b, key_nope[:end], preferred_element_type=f32) * scale
        dq_r = jnp.einsum("hqk,kd->qhd", ds_b, k_rope[:end], preferred_element_type=f32) * scale
        dq_r = rotate(dq_r, cosine[begin:end, None, :], -sine[begin:end, None, :])
        dq_parts.append(jnp.concatenate([dq_n, dq_r], axis=-1).astype(bf16))
        dk_nope = dk_nope.at[:end].add(
            jnp.einsum("hqk,qhd->khd", ds_b, qn, preferred_element_type=f32) * scale
        )
        dk_rope = dk_rope.at[:end].add(
            jnp.einsum("hqk,qhd->kd", ds_b, qr, preferred_element_type=f32) * scale
        )
        d_vals = d_vals.at[:end].add(
            jnp.einsum("hqk,qhd->khd", p_b, go, preferred_element_type=f32)
        )
    query_part = jnp.concatenate(dq_parts, axis=0)
    grads = jnp.concatenate([query_part, dk_nope.astype(bf16), d_vals.astype(bf16)], axis=-1)
    return (grads, rotate(dk_rope, cosine, -sine))


def local(query, latent, rope_key, latent_norm_gain, key_up_matrix, value_up_matrix, out_grad):
    f32 = jnp.float32
    bf16 = jnp.bfloat16
    tokens = latent.shape[1]
    width = PLAIN_HEAD_WIDTH + ROPE
    head_cols = ATTENTION_HEADS * PLAIN_HEAD_WIDTH
    lat = latent[0].astype(f32)
    inv_rms = lax.rsqrt(jnp.mean(lat * lat, axis=-1, keepdims=True) + eps)
    normed = lat * inv_rms
    nlat = (normed * latent_norm_gain).astype(bf16)
    stacked = jnp.stack([key_up_matrix, value_up_matrix])
    whole = lax.all_gather(stacked, "dp", axis=1, tiled=True)
    kv_tok = jnp.einsum("tc,gnc->tgn", nlat, whole, preferred_element_type=f32).astype(bf16)
    heads_query = query[0].reshape(tokens, ATTENTION_HEADS, width)
    key_nope = kv_tok[:, 0].reshape(tokens, ATTENTION_HEADS, PLAIN_HEAD_WIDTH)
    values = kv_tok[:, 1].reshape(tokens, ATTENTION_HEADS, VALUE_HEAD_WIDTH)
    d_out = out_grad[0].reshape(tokens, ATTENTION_HEADS, VALUE_HEAD_WIDTH)
    packed = jnp.concatenate([heads_query, key_nope, values, d_out], axis=2)
    arrived = lax.all_to_all(packed, "sp", split_axis=1, concat_axis=0, tiled=True)
    rope_full = lax.all_gather(rope_key[0], "sp", axis=0, tiled=True)
    grads_heads, rope_full_grad = attend_backward(arrived, rope_full)
    returned = lax.all_to_all(grads_heads, "sp", split_axis=0, concat_axis=1, tiled=True)
    rope_grad = lax.psum_scatter(rope_full_grad, "sp", scatter_dimension=0, tiled=True)
    query_grad = returned[:, :, :width].reshape(tokens, ATTENTION_HEADS * width)
    key_cols = returned[:, :, width : width + PLAIN_HEAD_WIDTH].reshape(tokens, head_cols)
    value_cols = returned[:, :, width + PLAIN_HEAD_WIDTH :].reshape(tokens, head_cols)
    dkv = jnp.stack([key_cols, value_cols], axis=1)
    d_nlat = jnp.einsum("tgn,gnc->tc", dkv, whole, preferred_element_type=f32)
    latents_all = lax.all_gather(nlat[None], "dp", axis=0, tiled=True)
    columns = lax.all_to_all(dkv[None], "dp", split_axis=3, concat_axis=0, tiled=True)
    partial_value = jnp.einsum("stgr,stc->grc", columns, latents_all, preferred_element_type=f32)
    weight_grads = lax.psum(partial_value, "sp")
    gain_grad = lax.psum(jnp.sum(d_nlat * normed, axis=0), ("sp", "dp"))
    scaled = d_nlat * latent_norm_gain
    latent_grad = inv_rms * (scaled - normed * jnp.mean(scaled * normed, axis=-1, keepdims=True))
    return (
        query_grad[None],
        latent_grad[None],
        rope_grad[None],
        weight_grads[0],
        weight_grads[1],
        gain_grad,
    )


def solution(mesh):
    in_specs = (
        P("dp", "sp", None),
        P("dp", "sp", None),
        P("dp", "sp", None),
        P(),
        P("dp", None),
        P("dp", None),
        P("dp", "sp", None),
    )
    out_specs = (
        P("dp", "sp", None),
        P("dp", "sp", None),
        P("dp", "sp", None),
        P("dp", None),
        P("dp", None),
        P(),
    )
    return jax.shard_map(local, mesh=mesh, in_specs=in_specs, out_specs=out_specs, check_vma=False)
```

profile of v0, /device:TPU:0, one launch (start us, length us, event | category | flops | bytes accessed | tf_op | source)
XLA Modules:
  0.0 738.0 jit_solution(6265751976223707838)
XLA Ops:
  7.2 3.1 pad_maximum_fusion.2
  10.9 1.4 copy.96
  12.3 3.9 reshape_squeeze.12
  16.4 55.1 %all-gather.4.cloned.1.call-done = bf16[2,2048,1024]{2,1,0:T(8,128)(2,1)} async-done(((bf16[2,512,1024]{2,1,0:T(8,128)(2,1)}), bf16[2,2048,1024]{2,1,0:T(8,128)(2,1)}) %all-gather.4.cloned.1.call-update) | async-done | bytes 8388624 | tf_op jit(solution)/shard_map/all_gather | solution.py:99
  71.5 6.2 convolution_convert_fusion
  80.0 2.4 copy.94
  82.4 2.2 copy.92
  84.6 3.1 copy.95
  87.8 5.6 pad_maximum_fusion
  93.4 4.0 copy.97
  97.4 5.6 all-to-all-start
  103.2 126.8 %all-gather = bf16[1,1536,32]{2,0,1:T(2,128)(2,1)S(1)} all-gather(bf16[1,192,32]{2,0,1:T(2,128)(2,1)S(1)} %copy.99), channel_id=2, replica_groups=mesh['sp'=8,'dp'=4] {'sp'}, dimensions={1}, use_global_device_ids=true | all-gather | bytes 110592 | tf_op jit(solution)/shard_map/all_gather | solution.py:107
  235.0 1.4 broadcast_compare_fusion
  236.4 8.3 %copy.98 = bf16[8,192,4,288]{1,0,3,2:T(8,128)(2,1)} copy(bf16[8,192,4,288]{3,1,2,0:T(8,128)(2,1)} %bitcast.8) | data formatting | bytes 7077888 | tf_op jit(solution)/shard_map/all_to_all | solution.py:106
  244.7 6.9 all_to_all.42
  254.7 3.3 fusion.152
  258.0 5.4 fusion.43
  263.4 3.1 multiply_reduce_fusion.2
  269.2 2.1 fusion.51
  271.3 1.7 fusion.46
  274.4 3.2 fusion.6
  277.6 2.0 fusion.153
  280.8 2.8 multiply_reduce_fusion.1
  283.7 9.7 %multiply_convert_fusion.1 = bf16[4,512,1024]{2,1,0:T(8,128)(2,1)S(1)} fusion(f32[4,512,1024]{2,1,0:T(8,128)S(1)} %get-tuple-element.177, f32[4,512]{1,0:T(4,128)S(1)} %get-tuple-element.176, f32[4,512,1024]{2,1,0:T(8,128)S(1)} %get-tuple-element.171, f32[4,512]{1,0:T(4,128)S(1)} %get-tuple-element.170), kind=kLoop, calls=%fused_computation.12 | loop fusion | flops 8388608 | bytes 20987904 | tf_op jit(solution)/shard_map/convert_element_type | solution.py:68
  293.4 2.1 fusion.54
  295.5 3.1 fusion.50
  298.7 1.8 fusion.114
  300.5 8.5 %fusion.4 = f32[4,512,1536]{2,1,0:T(8,128)} fusion(f32[1536,512,4]{0,1,2:T(8,128)S(1)} %fusion.114, pred[512,1536]{1,0:T(8,128)(4,1)S(1)} %copy-done.13, bf16[1536,4,288]{0,2,1:T(8,128)(2,1)} %copy-done.3), kind=kOutput, calls=%fused_computation.5 | convolution fusion | flops 412090368 | bytes 27000832 | tf_op jit(solution)/shard_map/qhd,khd->hqk/dot_general | solution.py:57
  309.1 14.9 %fusion.154 = (f32[4,512]{1,0:T(4,128)S(1)}, f32[4,512,1536]{2,1,0:T(8,128)}) fusion(f32[4,512,1536]{2,1,0:T(8,128)} %fusion.4), kind=kOutput, calls=%fused_computation.226 | output fusion | flops 6292991 | bytes 25174016 | tf_op jit(solution)/shard_map/sub | solution.py:65
  323.9 11.8 %multiply_reduce_fusion = (f32[4,512]{1,0:T(4,128)S(1)}, f32[4,512,1536]{2,1,0:T(8,128)}) fusion(f32[4,512,1536]{2,1,0:T(8,128)} %get-tuple-element.173, f32[4,512]{1,0:T(4,128)S(1)} %get-tuple-element.172, bf16[1536,4,288]{0,2,1:T(8,128)(2,1)} %copy-done.3), kind=kOutput, calls=%fused_computation.7 | convolution fusion | flops 412088320 | bytes 26230784 | tf_op jit(solution)/shard_map/qhd,khd->hqk/dot_general | solution.py:66
  335.7 6.0 multiply_convert_fusion
  341.8 4.5 fusion.52
  346.3 2.7 fusion.53
  348.9 1.3 scatter-add.24
  350.3 1.3 scatter-add.20
  351.6 11.2 %fusion.37 = f32[1536,4,64]{0,2,1:T(8,128)} fusion(f32[1536,4,64]{0,2,1:T(8,128)} %scatter-add.24, bf16[1536,4,288]{0,2,1:T(8,128)(2,1)} %copy-done.3, f32[4,512]{1,0:T(4,128)S(1)} %get-tuple-element.170, f32[4,512,1024]{2,1,0:T(8,128)} %copy-done.2), kind=kOutput, calls=%fused_computation.53 | convolution fusion | flops 274992128 | bytes 19144704 | tf_op jit(solution)/shard_map/hqk,qhd->khd/dot_general | solution.py:81
  362.8 4.4 fusion.42
  367.2 13.7 %fusion.22 = bf16[1536,4,64]{0,2,1:T(8,128)(2,1)} fusion(f32[1536,4,64]{0,2,1:T(8,128)} %fusion.37, bf16[1536,4,288]{0,2,1:T(8,128)(2,1)} %copy-done.3, f32[4,512]{1,0:T(4,128)S(1)} %get-tuple-element.172, f32[4,512,1536]{2,1,0:T(8,128)} %fusion.4), kind=kOutput, calls=%fused_computation.36 | convolution fusion | flops 412880384 | bytes 27795456 | tf_op jit(solution)/shard_map/hqk,qhd->khd/dot_general | solution.py:81
  381.0 4.6 fusion.21
  385.9 3.0 pad_maximum_fusion.1
  388.8 5.8 copy.107
  394.6 4.6 all-to-all-start.1
  401.9 64.4 %all-to-all-done.1 = bf16[1536,4,224]{2,1,0:T(4,128)(2,1)} async-done(((bf16[1536,4,224]{2,1,0:T(4,128)(2,1)}), bf16[1536,4,224]{2,1,0:T(4,128)(2,1)}, u32[]{:S(2)}, u32[]{:S(2)}) %all-to-all-start.1) | async-done | bytes 2752544 | tf_op jit(solution)/shard_map/all_to_all | solution.py:109
  466.3 2.3 copy.108
  468.8 2.8 fusion.149
  471.5 2.6 copy.111
  474.1 2.2 copy.113
  476.3 2.6 copy.112
  478.9 2.2 copy.114
  481.1 2.7 fusion.60
  483.8 6.1 copy.116
  489.8 4.4 all-to-all-start.2
  494.3 3.7 fusion.58
  498.0 4.0 fusion.26
  503.7 16.3 %all-to-all-done.2 = bf16[1,192,2,2048]{1,2,0,3:T(2,128)(2,1)} async-done(((bf16[1,192,2,2048]{1,2,0,3:T(2,128)(2,1)}), bf16[1,192,2,2048]{1,2,0,3:T(2,128)(2,1)}, u32[]{:S(2)}, u32[]{:S(2)}) %all-to-all-start.2) | async-done | bytes 1572896 | tf_op jit(solution)/shard_map/all_to_all | solution.py:117
  520.0 6.0 copy.118
  526.0 5.7 convolution_bitcast_fusion.1
  531.7 34.6 %reduce-scatter.4.cloned.1.call-done = f32[192,32]{1,0:T(8,128)} async-done(((f32[1536,32]{1,0:T(8,128)}), f32[192,32]{1,0:T(8,128)}) %reduce-scatter.4.cloned.1.call-update) | async-done | bytes 24592
  566.3 1.6 copy.130
  569.2 3.0 broadcast_in_dim_reshape.3
  572.2 6.3 fusion.72
  578.5 44.0 %psum.15 = f32[1024]{0:T(1024)} all-reduce(f32[1024]{0:T(1024)S(1)} %get-tuple-element.138), channel_id=1, replica_groups=mesh['sp'=8,'dp'=4] {'sp','dp'}, use_global_device_ids=true, to_apply=%region_14.15 | all-reduce | flops 1024 | bytes 8192 | tf_op jit(solution)/shard_map/psum | solution.py:120
  623.6 102.6 %all-reduce.5.cloned.1.call-done = f32[2,512,1024]{2,1,0:T(8,128)} async-done(((f32[2,512,1024]{2,1,0:T(8,128)}), f32[2,512,1024]{2,1,0:T(8,128)}) %all-reduce.5.cloned.1.call-update) | async-done | bytes 4194320 | tf_op jit(solution)/shard_map/psum | solution.py:119
  726.2 4.8 slice_bitcast_fusion
  (152 shorter events, 23.7 us)
Async XLA Ops:
  7.2 3.2 copy-start.32
  7.2 64.3 %all-gather.4.cloned.1.call-start = ((), (), s32[]{:S(2)}) async-start(), calls=%async_computation.4 | async-start | bytes 10485760 | tf_op jit(solution)/shard_map/all_gather | solution.py:99
  10.3 5.9 copy-start.10
  10.4 61.1 %copy-start.41 = (f32[1024]{0:T(1024)S(1)}, f32[1024]{0:T(1024)}, u32[]{:S(2)}) copy-start(f32[1024]{0:T(1024)} %param.34) | copy-start | bytes 12292
  16.4 55.1 %copy-start.44 = (f32[192]{0:T(256)}, f32[192]{0:T(256)S(1)}, u32[]{:S(2)}) copy-start(f32[192]{0:T(256)S(1)} %add_rsqrt_fusion) | copy-start | bytes 2308
  97.4 5.7 copy-start.43
  97.4 139.0 %all-to-all-start = ((bf16[192,32,288]{2,0,1:T(8,128)(2,1)}), bf16[192,32,288]{2,0,1:T(8,128)(2,1)}, u32[]{:S(2)}, u32[]{:S(2)}) async-start(bf16[192,32,288]{2,0,1:T(8,128)(2,1)} %copy.97), calls=%async_computation | async-start | bytes 9437184 | tf_op jit(solution)/shard_map/all_to_all | solution.py:106
  230.4 1.2 copy-start.46
  231.6 0.6 copy-start.28
  231.6 0.7 copy-start.30
  251.6 11.8 %copy-start.3 = (bf16[1536,4,288]{0,2,1:T(8,128)(2,1)}, bf16[1536,4,288]{0,2,1:T(8,128)(2,1)S(1)}, u32[]{:S(2)}) copy-start(bf16[1536,4,288]{0,2,1:T(8,128)(2,1)S(1)} %all_to_all.42) | copy-start | bytes 10616836
  251.6 1.0 copy-start.29
  251.6 1.1 copy-start.31
  251.6 2.0 copy-start.16
  251.6 2.0 copy-start.18
  251.6 2.0 copy-start.24
  252.8 0.7 copy-start.6
  252.8 0.8 copy-start.8
  254.7 3.3 copy-start.5
  263.4 3.4 copy-start.4
  266.8 1.2 copy-start.17
  266.8 1.2 copy-start.19
  268.0 5.0 copy-start.7
  268.0 5.0 copy-start.9
  273.0 1.3 copy-start.20
  277.6 3.3 copy-start.2
  293.4 5.2 copy-start.1
  298.7 1.8 copy-start.13
  323.9 11.8 %slice-start = ((s8[12582912]{0:T(1024)(128)(4,1)}), s8[4194304]{0:T(1024)(128)(4,1)S(1)}, s32[]{:S(2)}) async-start(s8[12582912]{0:T(1024)(128)(4,1)} %bitcast.187), calls=%async_computation.8 | async-start | bytes 8388608
  323.9 11.8 %slice-start.1 = ((s8[12582912]{0:T(1024)(128)(4,1)}), s8[4194304]{0:T(1024)(128)(4,1)S(1)}, s32[]{:S(2)}) async-start(s8[12582912]{0:T(1024)(128)(4,1)} %bitcast.187), calls=%async_computation.9 | async-start | bytes 8388608
  323.9 11.8 %slice-start.2 = ((s8[12582912]{0:T(1024)(128)(4,1)}), s8[4194304]{0:T(1024)(128)(4,1)S(1)}, s32[]{:S(2)}) async-start(s8[12582912]{0:T(1024)(128)(4,1)} %bitcast.187), calls=%async_computation.10 | async-start | bytes 8388608
  341.8 7.1 copy-start
  346.3 2.7 copy-start.34
  380.9 4.7 copy-start.21
  380.9 4.8 copy-start.39
  380.9 4.8 copy-start.40
  380.9 4.8 copy-start.22
  380.9 4.8 copy-start.37
  380.9 4.8 copy-start.38
  380.9 4.9 copy-start.23
  380.9 4.9 copy-start.35
  380.9 4.9 copy-start.36
  380.9 4.9 copy-start.25
  381.0 4.9 copy-start.26
  381.0 4.9 copy-start.27
  381.0 4.9 copy-start.33
  394.6 4.9 copy-start.11
  394.6 4.9 copy-start.42
  394.6 4.9 copy-start.45
  394.6 71.6 %all-to-all-start.1 = ((bf16[1536,4,224]{2,1,0:T(4,128)(2,1)}), bf16[1536,4,224]{2,1,0:T(4,128)(2,1)}, u32[]{:S(2)}, u32[]{:S(2)}) async-start(bf16[1536,4,224]{2,1,0:T(4,128)(2,1)} %copy.107), calls=%async_computation.1 | async-start | bytes 6291456 | tf_op jit(solution)/shard_map/all_to_all | solution.py:109
  399.2 126.8 %all-gather.6.cloned.1.call-start = ((), (), s32[]{:S(2)}) async-start(), calls=%async_computation.5 | async-start | bytes 1966080 | tf_op jit(solution)/shard_map/all_gather | solution.py:116
  489.8 30.2 %all-to-all-start.2 = ((bf16[1,192,2,2048]{1,2,0,3:T(2,128)(2,1)}), bf16[1,192,2,2048]{1,2,0,3:T(2,128)(2,1)}, u32[]{:S(2)}, u32[]{:S(2)}) async-start(bf16[1,192,2,2048]{1,2,0,3:T(2,128)(2,1)} %copy.116), calls=%async_computation.2 | async-start | bytes 4194304 | tf_op jit(solution)/shard_map/all_to_all | solution.py:117
  494.3 72.0 %reduce-scatter.4.cloned.1.call-start = ((), (), s32[]{:S(2)}) async-start(), calls=%async_computation.7 | async-start | bytes 884736
  498.0 4.0 copy-start.47
  503.6 222.6 %all-reduce.5.cloned.1.call-start = ((), (), s32[]{:S(2)}) async-start(), calls=%async_computation.6 | async-start | bytes 8388608 | tf_op jit(solution)/shard_map/psum | solution.py:119
  567.9 4.3 copy-start.12
  568.2 4.0 copy-start.14
  568.2 4.0 copy-start.15
Sparse Core Ops, SparseCore 0:
  10.5 60.9 all-gather.3
  401.6 19.9 all-gather.5
  503.8 62.4 reduce-scatter.3
  569.8 156.3 all-reduce.4
where the time goes:
time: 747 us; the launch traced here: 738 us
  waiting for transfers between devices  273 us (37%)
  blocking collectives  171 us (23%)
  matrix products  118 us (16%)
  local copies, waits for them, and re-layouts  87 us (12%)
  other arithmetic  59.6 us (8%)
  starting transfers between devices  15.1 us (2%)
  between operations  15 us (2%)
    all_gather x1, blocking collectives, local(): rope_full = lax.all_gather(rope_key[0], 'sp', axis=0, tiled=True)  127 us
    psum x1, waiting for transfers between devices, local(): weight_grads = lax.psum(partial_value, 'sp')  103 us
    all_to_all x1, waiting for transfers between devices, local(): lax.all_to_all(grads_heads, 'sp', split_axis=0, concat_axis=1, tiled=True)  64.4 us
    all_gather x1, waiting for transfers between devices, local(): whole = lax.all_gather(stacked, 'dp', axis=1, tiled=True)  55.1 us
    psum x1, blocking collectives, local(): gain_grad = lax.psum(jnp.sum(d_nlat * normed, axis=0), ('sp', 'dp'))  44 us
    unnamed x5, waiting for transfers between devices  34.6 us
    dot_general x3, matrix products, attend_backward(): jnp.einsum('hqk,qhd->khd', p_b, go, preferred_element_type=f32)  30.3 us
    sub x3, other arithmetic, attend_backward(): probs = jax.nn.softmax(scores, axis=-1)  20.1 us
  transfers between devices with their start and end apart: 7, of which 5 were waited for; matrix products, arithmetic and copies ran while one was open for 10% of the time, Pallas kernels for 0%

commit v1 on v0

--- a/solution.py
+++ b/solution.py
@@ -117,7 +117,7 @@
     columns = lax.all_to_all(dkv[None], "dp", split_axis=3, concat_axis=0, tiled=True)
     partial_value = jnp.einsum("stgr,stc->grc", columns, latents_all, preferred_element_type=f32)
     weight_grads = lax.psum(partial_value, "sp")
-    gain_grad = lax.psum(jnp.sum(d_nlat * normed, axis=0), ("sp", "dp"))
+    gain_grad = lax.psum(lax.psum(jnp.sum(d_nlat * normed, axis=0), "dp"), "sp")
     scaled = d_nlat * latent_norm_gain
     latent_grad = inv_rms * (scaled - normed * jnp.mean(scaled * normed, axis=-1, keepdims=True))
     return (

time: 747 us -> 747 us (level)
  blocking collectives: 171 us -> 153 us
  waiting for transfers between devices: 273 us -> 290 us
    psum x1 -> x2, blocking collectives: 44 us -> 26.1 us  [local(): gain_grad = lax.psum(lax.psum(jnp.sum(d_nlat * normed, axis=0), 'dp'), 'sp')]
    psum x1, waiting for transfers between devices: 103 us -> 120 us  [local(): weight_grads = lax.psum(partial_value, 'sp')]
where the time goes in v1:
time: 747 us; the launch traced here: 738 us
  waiting for transfers between devices  290 us (39%)
  blocking collectives  153 us (20%)
  matrix products  118 us (16%)
  local copies, waits for them, and re-layouts  87 us (12%)
  other arithmetic  59.7 us (8%)
  starting transfers between devices  15.1 us (2%)
  between operations  15 us (2%)
    all_gather x1, blocking collectives, local(): rope_full = lax.all_gather(rope_key[0], 'sp', axis=0, tiled=True)  127 us
    psum x1, waiting for transfers between devices, local(): weight_grads = lax.psum(partial_value, 'sp')  120 us
    all_to_all x1, waiting for transfers between devices, local(): lax.all_to_all(grads_heads, 'sp', split_axis=0, concat_axis=1, tiled=True)  64.4 us
    all_gather x1, waiting for transfers between devices, local(): whole = lax.all_gather(stacked, 'dp', axis=1, tiled=True)  55.1 us
    unnamed x5, waiting for transfers between devices  34.6 us
    dot_general x3, matrix products, attend_backward(): jnp.einsum('hqk,qhd->khd', p_b, go, preferred_element_type=f32)  30.4 us
    psum x2, blocking collectives, local(): gain_grad = lax.psum(lax.psum(jnp.sum(d_nlat * normed, axis=0), 'dp'), 'sp')  26.1 us
    sub x3, other arithmetic, attend_backward(): probs = jax.nn.softmax(scores, axis=-1)  20.1 us
  transfers between devices with their start and end apart: 7, of which 5 were waited for; matrix products, arithmetic and copies ran while one was open for 10% of the time, Pallas kernels for 0%

profile of v1, /device:TPU:0, one launch (start us, length us, event | category | flops | bytes accessed | tf_op | source)
XLA Modules:
  0.0 737.5 jit_solution(2584245670333585449)
XLA Ops:
  7.2 3.1 pad_maximum_fusion.2
  10.9 1.4 copy.96
  12.3 3.9 reshape_squeeze.12
  16.4 55.1 %all-gather.4.cloned.1.call-done = bf16[2,2048,1024]{2,1,0:T(8,128)(2,1)} async-done(((bf16[2,512,1024]{2,1,0:T(8,128)(2,1)}), bf16[2,2048,1024]{2,1,0:T(8,128)(2,1)}) %all-gather.4.cloned.1.call-update) | async-done | bytes 8388624 | tf_op jit(solution)/shard_map/all_gather | solution.py:99
  71.5 6.2 convolution_convert_fusion
  80.0 2.4 copy.94
  82.4 2.2 copy.92
  84.6 3.1 copy.95
  87.8 5.6 pad_maximum_fusion
  93.4 4.0 copy.97
  97.4 5.6 all-to-all-start
  103.1 126.8 %all-gather = bf16[1,1536,32]{2,0,1:T(2,128)(2,1)S(1)} all-gather(bf16[1,192,32]{2,0,1:T(2,128)(2,1)S(1)} %copy.99), channel_id=2, replica_groups=mesh['sp'=8,'dp'=4] {'sp'}, dimensions={1}, use_global_device_ids=true | all-gather | bytes 110592 | tf_op jit(solution)/shard_map/all_gather | solution.py:107
  235.0 1.4 broadcast_compare_fusion
  236.4 8.3 %copy.98 = bf16[8,192,4,288]{1,0,3,2:T(8,128)(2,1)} copy(bf16[8,192,4,288]{3,1,2,0:T(8,128)(2,1)} %bitcast.8) | data formatting | bytes 7077888 | tf_op jit(solution)/shard_map/all_to_all | solution.py:106
  244.7 6.9 all_to_all.42
  254.7 3.3 fusion.152
  257.9 5.4 fusion.43
  263.3 3.1 multiply_reduce_fusion.2
  269.2 2.1 fusion.51
  271.3 1.7 fusion.46
  274.3 3.2 fusion.6
  277.5 2.0 fusion.153
  279.5 1.3 copy-done.2
  280.8 2.8 multiply_reduce_fusion.1
  283.6 9.7 %multiply_convert_fusion.1 = bf16[4,512,1024]{2,1,0:T(8,128)(2,1)S(1)} fusion(f32[4,512,1024]{2,1,0:T(8,128)S(1)} %get-tuple-element.177, f32[4,512]{1,0:T(4,128)S(1)} %get-tuple-element.176, f32[4,512,1024]{2,1,0:T(8,128)S(1)} %get-tuple-element.171, f32[4,512]{1,0:T(4,128)S(1)} %get-tuple-element.170), kind=kLoop, calls=%fused_computation.12 | loop fusion | flops 8388608 | bytes 20987904 | tf_op jit(solution)/shard_map/convert_element_type | solution.py:68
  293.4 2.1 fusion.54
  295.5 3.1 fusion.50
  298.7 1.8 fusion.114
  300.5 8.5 %fusion.4 = f32[4,512,1536]{2,1,0:T(8,128)} fusion(f32[1536,512,4]{0,1,2:T(8,128)S(1)} %fusion.114, pred[512,1536]{1,0:T(8,128)(4,1)S(1)} %copy-done.13, bf16[1536,4,288]{0,2,1:T(8,128)(2,1)} %copy-done.3), kind=kOutput, calls=%fused_computation.5 | convolution fusion | flops 412090368 | bytes 27000832 | tf_op jit(solution)/shard_map/qhd,khd->hqk/dot_general | solution.py:57
  309.0 14.9 %fusion.154 = (f32[4,512]{1,0:T(4,128)S(1)}, f32[4,512,1536]{2,1,0:T(8,128)}) fusion(f32[4,512,1536]{2,1,0:T(8,128)} %fusion.4), kind=kOutput, calls=%fused_computation.226 | output fusion | flops 6292991 | bytes 25174016 | tf_op jit(solution)/shard_map/sub | solution.py:65
  323.9 11.8 %multiply_reduce_fusion = (f32[4,512]{1,0:T(4,128)S(1)}, f32[4,512,1536]{2,1,0:T(8,128)}) fusion(f32[4,512,1536]{2,1,0:T(8,128)} %get-tuple-element.173, f32[4,512]{1,0:T(4,128)S(1)} %get-tuple-element.172, bf16[1536,4,288]{0,2,1:T(8,128)(2,1)} %copy-done.3), kind=kOutput, calls=%fused_computation.7 | convolution fusion | flops 412088320 | bytes 26230784 | tf_op jit(solution)/shard_map/qhd,khd->hqk/dot_general | solution.py:66
  335.7 6.0 multiply_convert_fusion
  341.8 4.5 fusion.52
  346.3 2.7 fusion.53
  351.6 11.2 %fusion.37 = f32[1536,4,64]{0,2,1:T(8,128)} fusion(f32[1536,4,64]{0,2,1:T(8,128)} %scatter-add.24, bf16[1536,4,288]{0,2,1:T(8,128)(2,1)} %copy-done.3, f32[4,512]{1,0:T(4,128)S(1)} %get-tuple-element.170, f32[4,512,1024]{2,1,0:T(8,128)} %copy-done.2), kind=kOutput, calls=%fused_computation.53 | convolution fusion | flops 274992128 | bytes 19144704 | tf_op jit(solution)/shard_map/hqk,qhd->khd/dot_general | solution.py:81
  362.8 4.4 fusion.42
  367.2 13.7 %fusion.22 = bf16[1536,4,64]{0,2,1:T(8,128)(2,1)} fusion(f32[1536,4,64]{0,2,1:T(8,128)} %fusion.37, bf16[1536,4,288]{0,2,1:T(8,128)(2,1)} %copy-done.3, f32[4,512]{1,0:T(4,128)S(1)} %get-tuple-element.172, f32[4,512,1536]{2,1,0:T(8,128)} %fusion.4), kind=kOutput, calls=%fused_computation.36 | convolution fusion | flops 412880384 | bytes 27795456 | tf_op jit(solution)/shard_map/hqk,qhd->khd/dot_general | solution.py:81
  381.1 4.6 fusion.21
  386.0 3.0 pad_maximum_fusion.1
  388.9 5.8 copy.107
  394.7 4.6 all-to-all-start.1
  402.1 64.4 %all-to-all-done.1 = bf16[1536,4,224]{2,1,0:T(4,128)(2,1)} async-done(((bf16[1536,4,224]{2,1,0:T(4,128)(2,1)}), bf16[1536,4,224]{2,1,0:T(4,128)(2,1)}, u32[]{:S(2)}, u32[]{:S(2)}) %all-to-all-start.1) | async-done | bytes 2752544 | tf_op jit(solution)/shard_map/all_to_all | solution.py:109
  466.4 2.3 copy.108
  468.9 2.8 fusion.149
  471.7 2.6 copy.111
  474.3 2.2 copy.113
  476.5 2.6 copy.112
  479.1 2.2 copy.114
  481.3 2.7 fusion.60
  483.9 6.1 copy.116
  490.0 4.4 all-to-all-start.2
  494.5 3.7 fusion.58
  498.2 4.0 fusion.26
  503.9 16.3 %all-to-all-done.2 = bf16[1,192,2,2048]{1,2,0,3:T(2,128)(2,1)} async-done(((bf16[1,192,2,2048]{1,2,0,3:T(2,128)(2,1)}), bf16[1,192,2,2048]{1,2,0,3:T(2,128)(2,1)}, u32[]{:S(2)}, u32[]{:S(2)}) %all-to-all-start.2) | async-done | bytes 1572896 | tf_op jit(solution)/shard_map/all_to_all | solution.py:117
  520.2 6.0 copy.118
  526.2 5.7 convolution_bitcast_fusion.1
  531.9 34.6 %reduce-scatter.4.cloned.1.call-done = f32[192,32]{1,0:T(8,128)} async-done(((f32[1536,32]{1,0:T(8,128)}), f32[192,32]{1,0:T(8,128)}) %reduce-scatter.4.cloned.1.call-update) | async-done | bytes 24592
  566.5 1.6 copy.130
  569.4 3.0 broadcast_in_dim_reshape.3
  572.4 6.3 fusion.72
  578.7 6.1 psum.22
  584.8 20.0 %psum.23 = f32[1024]{0:T(1024)} all-reduce(f32[1024]{0:T(1024)S(1)} %psum.22), channel_id=1, replica_groups=mesh['sp'=8,'dp'=4] {'sp'}, use_global_device_ids=true, to_apply=%region_15.16 | all-reduce | flops 1024 | bytes 8192 | tf_op jit(solution)/shard_map/psum | solution.py:120
  605.9 119.8 %all-reduce.5.cloned.1.call-done = f32[2,512,1024]{2,1,0:T(8,128)} async-done(((f32[2,512,1024]{2,1,0:T(8,128)}), f32[2,512,1024]{2,1,0:T(8,128)}) %all-reduce.5.cloned.1.call-update) | async-done | bytes 4194320 | tf_op jit(solution)/shard_map/psum | solution.py:119
  725.7 4.8 slice_bitcast_fusion
  (153 shorter events, 25.1 us)
Async XLA Ops:
  7.2 3.2 copy-start.32
  7.2 64.3 %all-gather.4.cloned.1.call-start = ((), (), s32[]{:S(2)}) async-start(), calls=%async_computation.4 | async-start | bytes 10485760 | tf_op jit(solution)/shard_map/all_gather | solution.py:99
  10.3 5.9 copy-start.10
  10.4 61.1 %copy-start.41 = (f32[1024]{0:T(1024)S(1)}, f32[1024]{0:T(1024)}, u32[]{:S(2)}) copy-start(f32[1024]{0:T(1024)} %param.34) | copy-start | bytes 12292
  16.4 55.1 %copy-start.44 = (f32[192]{0:T(256)}, f32[192]{0:T(256)S(1)}, u32[]{:S(2)}) copy-start(f32[192]{0:T(256)S(1)} %add_rsqrt_fusion) | copy-start | bytes 2308
  97.4 5.7 copy-start.43
  97.4 139.0 %all-to-all-start = ((bf16[192,32,288]{2,0,1:T(8,128)(2,1)}), bf16[192,32,288]{2,0,1:T(8,128)(2,1)}, u32[]{:S(2)}, u32[]{:S(2)}) async-start(bf16[192,32,288]{2,0,1:T(8,128)(2,1)} %copy.97), calls=%async_computation | async-start | bytes 9437184 | tf_op jit(solution)/shard_map/all_to_all | solution.py:106
  230.4 1.2 copy-start.46
  231.6 0.6 copy-start.28
  231.6 0.7 copy-start.30
  251.6 11.7 %copy-start.3 = (bf16[1536,4,288]{0,2,1:T(8,128)(2,1)}, bf16[1536,4,288]{0,2,1:T(8,128)(2,1)S(1)}, u32[]{:S(2)}) copy-start(bf16[1536,4,288]{0,2,1:T(8,128)(2,1)S(1)} %all_to_all.42) | copy-start | bytes 10616836
  251.6 1.0 copy-start.29
  251.6 1.1 copy-start.31
  251.6 2.0 copy-start.16
  251.6 2.0 copy-start.18
  251.6 2.0 copy-start.24
  252.8 0.7 copy-start.6
  252.9 0.7 copy-start.8
  254.7 3.3 copy-start.5
  263.3 3.4 copy-start.4
  266.8 1.2 copy-start.17
  266.8 1.2 copy-start.19
  268.0 5.0 copy-start.7
  268.0 5.0 copy-start.9
  273.0 1.3 copy-start.20
  277.5 3.3 copy-start.2
  293.4 5.3 copy-start.1
  298.7 1.8 copy-start.13
  323.9 11.8 %slice-start = ((s8[12582912]{0:T(1024)(128)(4,1)}), s8[4194304]{0:T(1024)(128)(4,1)S(1)}, s32[]{:S(2)}) async-start(s8[12582912]{0:T(1024)(128)(4,1)} %bitcast.187), calls=%async_computation.8 | async-start | bytes 8388608
  323.9 11.8 %slice-start.1 = ((s8[12582912]{0:T(1024)(128)(4,1)}), s8[4194304]{0:T(1024)(128)(4,1)S(1)}, s32[]{:S(2)}) async-start(s8[12582912]{0:T(1024)(128)(4,1)} %bitcast.187), calls=%async_computation.9 | async-start | bytes 8388608
  323.9 11.8 %slice-start.2 = ((s8[12582912]{0:T(1024)(128)(4,1)}), s8[4194304]{0:T(1024)(128)(4,1)S(1)}, s32[]{:S(2)}) async-start(s8[12582912]{0:T(1024)(128)(4,1)} %bitcast.187), calls=%async_computation.10 | async-start | bytes 8388608
  341.8 7.2 copy-start
  346.3 2.7 copy-start.34
  381.0 4.7 copy-start.21
  381.0 4.8 copy-start.39
  381.0 4.8 copy-start.40
  381.0 4.8 copy-start.22
  381.0 4.8 copy-start.37
  381.0 4.8 copy-start.38
  381.0 4.9 copy-start.23
  381.0 4.9 copy-start.35
  381.0 4.9 copy-start.36
  381.0 4.9 copy-start.25
  381.0 4.9 copy-start.26
  381.1 4.9 copy-start.27
  381.1 4.9 copy-start.33
  394.7 4.9 copy-start.11
  394.7 4.9 copy-start.42
  394.7 4.9 copy-start.45
  394.7 71.7 %all-to-all-start.1 = ((bf16[1536,4,224]{2,1,0:T(4,128)(2,1)}), bf16[1536,4,224]{2,1,0:T(4,128)(2,1)}, u32[]{:S(2)}, u32[]{:S(2)}) async-start(bf16[1536,4,224]{2,1,0:T(4,128)(2,1)} %copy.107), calls=%async_computation.1 | async-start | bytes 6291456 | tf_op jit(solution)/shard_map/all_to_all | solution.py:109
  399.3 126.9 %all-gather.6.cloned.1.call-start = ((), (), s32[]{:S(2)}) async-start(), calls=%async_computation.5 | async-start | bytes 1966080 | tf_op jit(solution)/shard_map/all_gather | solution.py:116
  490.0 30.2 %all-to-all-start.2 = ((bf16[1,192,2,2048]{1,2,0,3:T(2,128)(2,1)}), bf16[1,192,2,2048]{1,2,0,3:T(2,128)(2,1)}, u32[]{:S(2)}, u32[]{:S(2)}) async-start(bf16[1,192,2,2048]{1,2,0,3:T(2,128)(2,1)} %copy.116), calls=%async_computation.2 | async-start | bytes 4194304 | tf_op jit(solution)/shard_map/all_to_all | solution.py:117
  494.4 72.0 %reduce-scatter.4.cloned.1.call-start = ((), (), s32[]{:S(2)}) async-start(), calls=%async_computation.7 | async-start | bytes 884736
  498.2 4.0 copy-start.47
  503.8 221.9 %all-reduce.5.cloned.1.call-start = ((), (), s32[]{:S(2)}) async-start(), calls=%async_computation.6 | async-start | bytes 8388608 | tf_op jit(solution)/shard_map/psum | solution.py:119
  568.1 4.3 copy-start.12
  568.4 4.0 copy-start.14
  568.4 4.0 copy-start.15
Sparse Core Ops, SparseCore 0:
  10.5 60.9 all-gather.3
  401.7 19.9 all-gather.5
  503.9 62.4 reduce-scatter.3
  570.0 155.6 all-reduce.4
